TPU v7x, 32 devices: a whole 2x2x4 slice. The times are simulated.
32 devices in a mesh: fs: 4 (over z), tp: 8 (over y, x, core).
Axes of the slice: x: 2, y: 2, z: 4, core: 2. Of those that a mesh axis runs over, the one named last changes fastest.
Arguments:
- grad_gate: float32 [2112, 5632], P('fs', 'tp'), may hold values from -45 to 45
- grad_up: float32 [2112, 5632], P('fs', 'tp'), may hold values from -45 to 45
- moment_gate: float32 [2112, 5632], P('fs', 'tp'), may hold values from -6 to 6
- moment_up: float32 [2112, 5632], P('fs', 'tp'), may hold values from -6 to 6
Outputs:
- moment_gate_next: float32 [2112, 5632], P('fs', 'tp')
- moment_up_next: float32 [2112, 5632], P('fs', 'tp')
- update_gate: float32 [2112, 5632], P('fs', 'tp')
- update_up: float32 [2112, 5632], P('fs', 'tp')
All inputs are finite; a program needn't handle non-finite values.
Results may differ from a plain program's by a relative error of at most 0.0019.
The roundings to bfloat16 on the way count: a program that leaves them out, or rounds other values in their place, can miss the bound.
Values may be sent and summed in bfloat16 or wider, within the bound.
A program may use at most 64 MiB of HBM per device.

v0:
```python
import jax
import jax.numpy as jnp
from jax import lax
from jax.sharding import PartitionSpec as P

FF = 5632
ITERS = 3


BETA = 0.95
EPS = 1e-06


def multiply(left_low, right_low):
    left_rows = lax.all_gather(left_low, "fs", axis=1, tiled=True)
    return jnp.dot(
        left_rows,
        lax.all_gather(right_low, "tp", axis=0, tiled=True),
        preferred_element_type=jnp.float32,
    )


def local(grad_gate, grad_up, moment_gate, moment_up):
    moment_gate_next = BETA * moment_gate + grad_gate
    moment_up_next = BETA * moment_up + grad_up
    low_gate = moment_gate_next.astype(jnp.bfloat16)
    low_up = moment_up_next.astype(jnp.bfloat16)
    trace_local = jnp.sum(jnp.square(low_gate.astype(jnp.float32))) + jnp.sum(
        jnp.square(low_up.astype(jnp.float32))
    )
    columns_gate, columns_up = (
        lax.all_gather(low_gate, "fs", axis=0, tiled=True),
        lax.all_gather(low_up, "fs", axis=0, tiled=True),
    )
    rows_dev = low_gate.shape[0]
    width = columns_gate.shape[0]
    own_rows = width // lax.axis_size("tp")
    block_gate = columns_gate
    block_up = columns_up
    gram = lax.psum_scatter(
        jnp.einsum("ik,jk->ij", block_gate, low_gate, preferred_element_type=jnp.float32)
        + jnp.einsum("ik,jk->ij", block_up, low_up, preferred_element_type=jnp.float32),
        "tp",
        scatter_dimension=0,
        tiled=True,
    )
    square_local = jnp.sum(gram * gram)
    trace_total, square_total = lax.psum((trace_local, square_local), ("fs", "tp"))
    spectral = 2.0 * square_total / (trace_total + EPS)
    current = gram / spectral
    row_index = lax.axis_index("tp") * own_rows + lax.broadcasted_iota(
        jnp.int32, (own_rows, rows_dev), 0
    )
    col_index = lax.axis_index("fs") * rows_dev + lax.broadcasted_iota(
        jnp.int32, (own_rows, rows_dev), 1
    )
    identity = (row_index == col_index).astype(jnp.float32)
    product_low = None
    for iteration in range(ITERS):
        poly_low = (1.5 * identity - 0.5 * current).astype(jnp.bfloat16)
        final_turn = iteration == ITERS - 1
        square_low = None
        if iteration == 0:
            product_low = poly_low
            square_low = multiply(poly_low, poly_low).astype(jnp.bfloat16)
        elif final_turn:
            product_low = multiply(product_low, poly_low).astype(jnp.bfloat16)
        else:
            product_low = multiply(product_low, poly_low).astype(jnp.bfloat16)
            square_low = multiply(poly_low, poly_low).astype(jnp.bfloat16)
        if not final_turn:
            current = multiply(current.astype(jnp.bfloat16), square_low)
    factor = jnp.sqrt(2.0 * FF / spectral)
    segment = lax.all_gather(product_low, "tp", axis=0, tiled=True)
    block_gate = columns_gate
    block_up = columns_up
    ortho_gate = jnp.einsum("jr,jc->rc", segment, block_gate, preferred_element_type=jnp.float32)
    ortho_up = jnp.einsum("jr,jc->rc", segment, block_up, preferred_element_type=jnp.float32)
    return (moment_gate_next, moment_up_next, ortho_gate * factor, ortho_up * factor)


def solution(mesh):
    in_specs = (P("fs", "tp"), P("fs", "tp"), P("fs", "tp"), P("fs", "tp"))
    out_specs = (P("fs", "tp"), P("fs", "tp"), P("fs", "tp"), P("fs", "tp"))
    return jax.shard_map(local, mesh=mesh, in_specs=in_specs, out_specs=out_specs, check_vma=False)
```

profile of v0, /device:TPU:0, one launch (start us, length us, event | category | flops | bytes accessed | tf_op | source)
XLA Modules:
  0.0 640.1 jit_solution(17345301320345391013)
XLA Ops:
  7.2 4.4 multiply_reduce_fusion.1
  11.7 0.0 all-gather.21.cloned.1.call-start
  11.7 4.0 multiply_reduce_fusion
  15.7 0.0 reduce-scatter.4.cloned.1.call-start
  15.8 63.8 %all-gather.19.cloned.1.call-done = bf16[2112,704]{1,0:T(8,128)(2,1)} async-done(((bf16[528,704]{1,0:T(8,128)(2,1)}), bf16[2112,704]{1,0:T(8,128)(2,1)}) %all-gather.19.cloned.1.call-update) | async-done | bytes 2973712 | tf_op jit(solution)/shard_map/all_gather | solution.py:32
  79.6 7.0 %fusion.5 = f32[2112,528]{1,0:T(8,128)} fusion(bf16[2112,704]{1,0:T(8,128)(2,1)} %all-gather.19.cloned.1.call-done, bf16[528,704]{1,0:T(8,128)(2,1)S(1)} %copy-done), kind=kOutput, calls=%fused_computation.25 | convolution fusion | flops 1570111488 | bytes 8177664 | tf_op jit(solution)/shard_map/ik,jk->ij/dot_general | solution.py:41
  86.6 58.9 %all-gather.21.cloned.1.call-done = bf16[2112,704]{1,0:T(8,128)(2,1)} async-done(((bf16[528,704]{1,0:T(8,128)(2,1)}), bf16[2112,704]{1,0:T(8,128)(2,1)}) %all-gather.21.cloned.1.call-update) | async-done | bytes 2973712 | tf_op jit(solution)/shard_map/all_gather | solution.py:33
  145.5 8.6 %convolution_add_fusion = f32[2112,528]{1,0:T(8,128)} fusion(f32[2112,528]{1,0:T(8,128)} %fusion.5, bf16[2112,704]{1,0:T(8,128)(2,1)} %all-gather.21.cloned.1.call-done, bf16[528,704]{1,0:T(8,128)(2,1)S(1)} %copy-done.1), kind=kOutput, calls=%fused_computation | convolution fusion | flops 1571226624 | bytes 12638208 | tf_op jit(solution)/shard_map/ik,jk->ij/dot_general | solution.py:42
  154.1 0.0 all-gather.35.cloned.1.call-start
  155.4 54.1 %reduce-scatter.4.cloned.1.call-done = f32[264,528]{1,0:T(8,128)} async-done(((f32[2112,528]{1,0:T(8,128)}), f32[264,528]{1,0:T(8,128)}) %reduce-scatter.4.cloned.1.call-update) | async-done | bytes 557584
  209.5 1.9 multiply_reduce_fusion.2
  211.4 39.5 %all-reduce.1 = (f32[]{:T(128)}, f32[]{:T(128)}) all-reduce(f32[]{:T(128)} %multiply_reduce_fusion.2, f32[]{:T(128)S(6)} %add.42), channel_id=1, replica_groups=mesh['fs'=4,'tp'=8] {'fs','tp'}, use_global_device_ids=true, to_apply=%region_2.0 | all-reduce | flops 2 | bytes 16 | tf_op jit(solution)/shard_map/psum | solution.py:48
  252.2 2.1 convert_bitcast_fusion.1
  254.4 0.5 all-gather.23.cloned.1.call-update
  255.0 0.5 all-gather.37.cloned.1.call-update
  255.6 33.1 %all-gather.35.cloned.1.call-done = bf16[4,528,264]{1,2,0:T(8,128)(2,1)} async-done(((bf16[1,528,264]{1,2,0:T(8,128)(2,1)}), bf16[4,528,264]{1,2,0:T(8,128)(2,1)}) %all-gather.35.cloned.1.call-update) | async-done | bytes 1115152 | tf_op jit(solution)/shard_map/all_gather | solution.py:15
  288.6 1.9 copy.13
  290.5 0.8 reshape.9
  291.3 29.0 %all-gather.23.cloned.1.call-done = bf16[2112,528]{1,0:T(8,128)(2,1)} async-done(((bf16[264,528]{1,0:T(8,128)(2,1)}), bf16[2112,528]{1,0:T(8,128)(2,1)}) %all-gather.23.cloned.1.call-update) | async-done | bytes 2230288 | tf_op jit(solution)/shard_map/all_gather | solution.py:18
  320.4 3.6 convolution_convert_fusion.3
  324.0 0.2 all-gather.43.cloned.1.call-start
  324.2 31.4 %all-gather.37.cloned.1.call-done = bf16[4,528,264]{1,2,0:T(8,128)(2,1)} async-done(((bf16[1,528,264]{1,2,0:T(8,128)(2,1)}), bf16[4,528,264]{1,2,0:T(8,128)(2,1)}) %all-gather.37.cloned.1.call-update) | async-done | bytes 1115152 | tf_op jit(solution)/shard_map/all_gather | solution.py:15
  355.6 1.9 copy.14
  357.5 1.8 reshape.11
  359.3 28.2 %all-gather.25.cloned.1.call-done = bf16[2112,528]{1,0:T(8,128)(2,1)} async-done(((bf16[264,528]{1,0:T(8,128)(2,1)}), bf16[2112,528]{1,0:T(8,128)(2,1)}) %all-gather.25.cloned.1.call-update) | async-done | bytes 2230288 | tf_op jit(solution)/shard_map/all_gather | solution.py:18
  387.5 4.1 convert_bitcast_fusion
  391.7 0.7 all-gather.27.cloned.1.call-update
  392.4 0.5 all-gather.41.cloned.1.call-update
  393.0 32.0 %all-gather.43.cloned.1.call-done = bf16[4,528,264]{1,2,0:T(8,128)(2,1)} async-done(((bf16[1,528,264]{1,2,0:T(8,128)(2,1)}), bf16[4,528,264]{1,2,0:T(8,128)(2,1)}) %all-gather.43.cloned.1.call-update) | async-done | bytes 1115152 | tf_op jit(solution)/shard_map/all_gather | solution.py:15
  425.0 1.9 copy.17
  426.8 1.8 reshape.17
  428.7 27.6 %all-gather.27.cloned.1.call-done = bf16[2112,528]{1,0:T(8,128)(2,1)} async-done(((bf16[264,528]{1,0:T(8,128)(2,1)}), bf16[2112,528]{1,0:T(8,128)(2,1)}) %all-gather.27.cloned.1.call-update) | async-done | bytes 2230288 | tf_op jit(solution)/shard_map/all_gather | solution.py:18
  456.3 4.0 convolution_convert_fusion.1
  460.3 3.6 fusion.2
  464.0 27.5 %all-gather.41.cloned.1.call-done = bf16[4,528,264]{1,2,0:T(8,128)(2,1)} async-done(((bf16[1,528,264]{1,2,0:T(8,128)(2,1)}), bf16[4,528,264]{1,2,0:T(8,128)(2,1)}) %all-gather.41.cloned.1.call-update) | async-done | bytes 1115152 | tf_op jit(solution)/shard_map/all_gather | solution.py:15
  491.5 1.9 copy.16
  493.4 0.8 reshape.15
  494.2 28.6 %all-gather.29.cloned.1.call-done = bf16[2112,528]{1,0:T(8,128)(2,1)} async-done(((bf16[264,528]{1,0:T(8,128)(2,1)}), bf16[2112,528]{1,0:T(8,128)(2,1)}) %all-gather.29.cloned.1.call-update) | async-done | bytes 2230288 | tf_op jit(solution)/shard_map/all_gather | solution.py:18
  522.9 3.6 fusion.1
  526.5 0.3 all-gather.33.cloned.1.call-start
  526.8 31.3 %all-gather.39.cloned.1.call-done = bf16[4,528,264]{1,2,0:T(8,128)(2,1)} async-done(((bf16[1,528,264]{1,2,0:T(8,128)(2,1)}), bf16[4,528,264]{1,2,0:T(8,128)(2,1)}) %all-gather.39.cloned.1.call-update) | async-done | bytes 1115152 | tf_op jit(solution)/shard_map/all_gather | solution.py:15
  558.1 1.9 copy.15
  560.0 0.8 reshape.13
  560.8 29.2 %all-gather.31.cloned.1.call-done = bf16[2112,528]{1,0:T(8,128)(2,1)} async-done(((bf16[264,528]{1,0:T(8,128)(2,1)}), bf16[2112,528]{1,0:T(8,128)(2,1)}) %all-gather.31.cloned.1.call-update) | async-done | bytes 2230288 | tf_op jit(solution)/shard_map/all_gather | solution.py:18
  590.0 3.6 convolution_convert_fusion
  593.7 30.4 %all-gather.33.cloned.1.call-done = bf16[2112,528]{1,0:T(8,128)(2,1)} async-done(((bf16[264,528]{1,0:T(8,128)(2,1)}), bf16[2112,528]{1,0:T(8,128)(2,1)}) %all-gather.33.cloned.1.call-update) | async-done | bytes 2230288 | tf_op jit(solution)/shard_map/all_gather | solution.py:74
  624.1 6.1 convolution_multiply_fusion
  630.2 3.3 convolution_multiply_fusion.1
  (31 shorter events, 0.6 us)
Async XLA Ops:
  7.2 72.4 %all-gather.19.cloned.1.call-start = ((), (), s32[]{:S(2)}) async-start(), calls=%async_computation.1 | async-start | bytes 4055040 | tf_op jit(solution)/shard_map/all_gather | solution.py:32
  7.2 4.5 copy-start.2
  11.7 67.9 %copy-start = (bf16[528,704]{1,0:T(8,128)(2,1)S(1)}, bf16[528,704]{1,0:T(8,128)(2,1)}, u32[]{:S(2)}) copy-start(bf16[528,704]{1,0:T(8,128)(2,1)} %get-tuple-element.10) | copy-start | bytes 2230276
  11.7 133.8 %all-gather.21.cloned.1.call-start = ((), (), s32[]{:S(2)}) async-start(), calls=%async_computation.2 | async-start | bytes 4055040 | tf_op jit(solution)/shard_map/all_gather | solution.py:33
  15.7 129.8 %copy-start.1 = (bf16[528,704]{1,0:T(8,128)(2,1)S(1)}, bf16[528,704]{1,0:T(8,128)(2,1)}, u32[]{:S(2)}) copy-start(bf16[528,704]{1,0:T(8,128)(2,1)} %get-tuple-element.7) | copy-start | bytes 2230276
  15.7 193.8 %reduce-scatter.4.cloned.1.call-start = ((), (), s32[]{:S(2)}) async-start(), calls=%async_computation.14 | async-start | bytes 6082560
  154.1 134.5 %all-gather.35.cloned.1.call-start = ((), (), s32[]{:S(2)}) async-start(), calls=%async_computation.9 | async-start | bytes 1689600 | tf_op jit(solution)/shard_map/all_gather | solution.py:15
  254.3 66.0 %all-gather.23.cloned.1.call-start = ((), (), s32[]{:S(2)}) async-start(), calls=%async_computation.3 | async-start | bytes 3041280 | tf_op jit(solution)/shard_map/all_gather | solution.py:18
  254.9 100.7 %all-gather.37.cloned.1.call-start = ((), (), s32[]{:S(2)}) async-start(), calls=%async_computation.10 | async-start | bytes 1689600 | tf_op jit(solution)/shard_map/all_gather | solution.py:15
  255.5 132.0 %all-gather.25.cloned.1.call-start = ((), (), s32[]{:S(2)}) async-start(), calls=%async_computation.4 | async-start | bytes 3041280 | tf_op jit(solution)/shard_map/all_gather | solution.py:18
  324.0 101.0 %all-gather.43.cloned.1.call-start = ((), (), s32[]{:S(2)}) async-start(), calls=%async_computation.13 | async-start | bytes 1689600 | tf_op jit(solution)/shard_map/all_gather | solution.py:15
  391.6 64.7 %all-gather.27.cloned.1.call-start = ((), (), s32[]{:S(2)}) async-start(), calls=%async_computation.5 | async-start | bytes 3041280 | tf_op jit(solution)/shard_map/all_gather | solution.py:18
  392.4 99.2 %all-gather.41.cloned.1.call-start = ((), (), s32[]{:S(2)}) async-start(), calls=%async_computation.12 | async-start | bytes 1689600 | tf_op jit(solution)/shard_map/all_gather | solution.py:15
  392.9 129.9 %all-gather.29.cloned.1.call-start = ((), (), s32[]{:S(2)}) async-start(), calls=%async_computation.6 | async-start | bytes 3041280 | tf_op jit(solution)/shard_map/all_gather | solution.py:18
  460.3 97.8 %all-gather.39.cloned.1.call-start = ((), (), s32[]{:S(2)}) async-start(), calls=%async_computation.11 | async-start | bytes 1689600 | tf_op jit(solution)/shard_map/all_gather | solution.py:15
  464.0 126.0 %all-gather.31.cloned.1.call-start = ((), (), s32[]{:S(2)}) async-start(), calls=%async_computation.7 | async-start | bytes 3041280 | tf_op jit(solution)/shard_map/all_gather | solution.py:18
  526.5 97.6 %all-gather.33.cloned.1.call-start = ((), (), s32[]{:S(2)}) async-start(), calls=%async_computation.8 | async-start | bytes 3041280 | tf_op jit(solution)/shard_map/all_gather | solution.py:74
  593.7 36.5 %copy-start.3 = (bf16[2112,704]{1,0:T(8,128)(2,1)S(1)}, bf16[2112,704]{1,0:T(8,128)(2,1)}, u32[]{:S(2)}) copy-start(bf16[2112,704]{1,0:T(8,128)(2,1)} %all-gather.19.cloned.1.call-done) | copy-start | bytes 8921092
  624.1 6.1 copy-start.4
Sparse Core Ops, SparseCore 0:
  11.8 67.7 all-gather.18
  81.7 63.6 all-gather.20
  154.2 55.2 reduce-scatter.3
  254.5 34.1 all-gather.34
  290.9 29.3 all-gather.22
  322.4 33.2 all-gather.36
  358.1 29.3 all-gather.24
  391.7 33.2 all-gather.42
  426.9 29.3 all-gather.26
  458.3 33.2 all-gather.40
  493.4 29.3 all-gather.28
  524.8 33.2 all-gather.38
  560.5 29.3 all-gather.30
  593.7 30.3 all-gather.32
where the time goes:
time: 641 us; the launch traced here: 640 us
  waiting for transfers between devices  508 us (79%)
  matrix products  47.6 us (7%)
  blocking collectives  39.5 us (6%)
  between operations  16.7 us (3%)
  local copies, waits for them, and re-layouts  15.4 us (2%)
  other arithmetic  12.4 us (2%)
    all_gather x5, waiting for transfers between devices, multiply(): left_rows = lax.all_gather(left_low, 'fs', axis=1, tiled=True)  155 us
    all_gather x5, waiting for transfers between devices, multiply(): lax.all_gather(right_low, 'tp', axis=0, tiled=True)  143 us
    all_gather x1, waiting for transfers between devices, local(): lax.all_gather(low_gate, 'fs', axis=0, tiled=True)  63.8 us
    all_gather x1, waiting for transfers between devices, local(): lax.all_gather(low_up, 'fs', axis=0, tiled=True)  58.9 us
    unnamed x15, waiting for transfers between devices  56.5 us
    psum x1, blocking collectives, local(): lax.psum((trace_local, square_local), ('fs', 'tp'))  39.5 us
    all_gather x1, waiting for transfers between devices, local(): segment = lax.all_gather(product_low, 'tp', axis=0, tiled=True)  30.4 us
    dot_general x6, matrix products, multiply(): jnp.dot(left_rows, lax.all_gather(right_low, 'tp', axis=0, tiled=True), p...  22.6 us
  transfers between devices with their start and end apart: 14, of which 14 were waited for; matrix products, arithmetic and copies ran while one was open for 6% of the time, Pallas kernels for 0%

commit v1 on v0

--- a/solution.py
+++ b/solution.py
@@ -1,9 +1,12 @@
+import functools
+
 import jax
 import jax.numpy as jnp
 from jax import lax
+from jax.experimental import pallas as pl
+from jax.experimental.pallas import tpu as pltpu
 from jax.sharding import PartitionSpec as P
 
-FF = 5632
 ITERS = 3
 
 
@@ -20,7 +23,8 @@
     )
 
 
-def local(grad_gate, grad_up, moment_gate, moment_up):
+def local_small(grad_gate, grad_up, moment_gate, moment_up):
+    hidden = grad_gate.shape[1] * lax.axis_size("tp")
     moment_gate_next = BETA * moment_gate + grad_gate
     moment_up_next = BETA * moment_up + grad_up
     low_gate = moment_gate_next.astype(jnp.bfloat16)
@@ -70,7 +74,7 @@
             square_low = multiply(poly_low, poly_low).astype(jnp.bfloat16)
         if not final_turn:
             current = multiply(current.astype(jnp.bfloat16), square_low)
-    factor = jnp.sqrt(2.0 * FF / spectral)
+    factor = jnp.sqrt(2.0 * hidden / spectral)
     segment = lax.all_gather(product_low, "tp", axis=0, tiled=True)
     block_gate = columns_gate
     block_up = columns_up
@@ -79,6 +83,535 @@
     return (moment_gate_next, moment_up_next, ortho_gate * factor, ortho_up * factor)
 
 
+MESH = pl.DeviceIdType.MESH
+
+
+def remote(src, dst, send_sem, recv_sem, z, t):
+    return pltpu.make_async_remote_copy(
+        src_ref=src,
+        dst_ref=dst,
+        send_sem=send_sem,
+        recv_sem=recv_sem,
+        device_id=(z, t),
+        device_id_type=MESH,
+    )
+
+
+def gather_kernel(
+    planes, ranks, low_ref, vec_ref, cols_ref, gram_ref, vecs_ref, z_send, z_recv, v_send, v_recv
+):
+    z, t = lax.axis_index("fs"), lax.axis_index("tp")
+    offsets = [(a, b) for a in range(planes) for b in range(ranks) if a or b]
+    barrier = pltpu.get_barrier_semaphore()
+    for a, b in offsets:
+        pl.semaphore_signal(
+            barrier,
+            inc=1,
+            device_id=(lax.rem(z + a, planes), lax.rem(t + b, ranks)),
+            device_id_type=MESH,
+        )
+    pl.semaphore_wait(barrier, len(offsets))
+
+    def right(step):
+        block = z - step
+        src = low_ref if step == 0 else cols_ref.at[block]
+        copy = remote(src, cols_ref.at[block], z_send.at[0, step], z_recv.at[0, step], z + 1, t)
+        return copy, (block >= 0) & (z + 1 < planes)
+
+    def left(step):
+        block = z + step
+        src = low_ref if step == 0 else cols_ref.at[block]
+        copy = remote(src, cols_ref.at[block], z_send.at[1, step], z_recv.at[1, step], z - 1, t)
+        return copy, (block < planes) & (z >= 1)
+
+    def start(make, step):
+        copy, valid = make(step)
+
+        @pl.when(valid)
+        def _():
+            copy.start()
+
+    def product(block):
+        tile = 176 if low_ref.shape[0] % 176 == 0 else low_ref.shape[0]
+
+        @pl.loop(0, low_ref.shape[0] // tile)
+        def _(i):
+            rows = pl.ds(pl.multiple_of(i * tile, 16), tile)
+            gram_ref[block, rows, :] = lax.dot_general(
+                cols_ref[block, rows, :],
+                low_ref[...],
+                (((1,), (1,)), ((), ())),
+                preferred_element_type=jnp.float32,
+            )
+
+    start(right, 0)
+    start(left, 0)
+    small = []
+    for a, b in offsets:
+        copy = remote(
+            vec_ref,
+            vecs_ref.at[z, t],
+            v_send.at[a, b],
+            v_recv.at[a, b],
+            lax.rem(z + a, planes),
+            lax.rem(t + b, ranks),
+        )
+        copy.start()
+        small.append(copy)
+    vecs_ref[z, t] = vec_ref[...]
+    cols_ref[z] = low_ref[...]
+    product(z)
+    for step in range(planes - 1):
+        from_left = z - 1 - step
+        from_right = z + 1 + step
+
+        @pl.when(from_left >= 0)
+        def _():
+            remote(
+                low_ref, cols_ref.at[from_left], z_send.at[0, step], z_recv.at[0, step], z, t
+            ).wait_recv()
+
+        if step + 1 < planes - 1:
+            start(right, step + 1)
+
+        @pl.when(from_right < planes)
+        def _():
+            remote(
+                low_ref, cols_ref.at[from_right], z_send.at[1, step], z_recv.at[1, step], z, t
+            ).wait_recv()
+
+        if step + 1 < planes - 1:
+            start(left, step + 1)
+
+        @pl.when(from_left >= 0)
+        def _():
+            product(from_left)
+
+        @pl.when(from_right < planes)
+        def _():
+            product(from_right)
+
+    for make in (right, left):
+        for step in range(planes - 1):
+            copy, valid = make(step)
+
+            @pl.when(valid)
+            def _():
+                copy.wait_send()
+
+    for copy in small:
+        copy.wait()
+
+
+def gather_and_gram(low, vec, planes, ranks):
+    rows, depth = low.shape
+    vmem = pl.BlockSpec(memory_space=pltpu.VMEM)
+    return pl.pallas_call(
+        functools.partial(gather_kernel, planes, ranks),
+        out_shape=(
+            jax.ShapeDtypeStruct((planes, rows, depth), jnp.bfloat16),
+            jax.ShapeDtypeStruct((planes, rows, rows), jnp.float32),
+            jax.ShapeDtypeStruct((planes, ranks, 1, rows), jnp.float32),
+        ),
+        in_specs=[vmem, vmem],
+        out_specs=(vmem, vmem, vmem),
+        scratch_shapes=[
+            pltpu.SemaphoreType.DMA((2, planes)),
+            pltpu.SemaphoreType.DMA((2, planes)),
+            pltpu.SemaphoreType.DMA((planes, ranks)),
+            pltpu.SemaphoreType.DMA((planes, ranks)),
+        ],
+        compiler_params=pltpu.CompilerParams(
+            collective_id=1, has_side_effects=True, vmem_limit_bytes=40 << 20
+        ),
+        cost_estimate=pl.CostEstimate(
+            flops=2 * planes * rows * rows * depth, bytes_accessed=100 << 20, transcendentals=0
+        ),
+    )(low, vec)
+
+
+def spread_kernel(
+    planes,
+    gram_ref,
+    full_ref,
+    halves,
+    part,
+    landed,
+    h_send,
+    h_recv,
+    p_send,
+    p_recv,
+    z_send,
+    z_recv,
+    a_send,
+    a_recv,
+    b_send,
+    b_recv,
+    d_send,
+    d_recv,
+):
+    z, t = lax.axis_index("fs"), lax.axis_index("tp")
+    core, chip = lax.rem(t, 2), t // 2
+    cx, cy = lax.rem(chip, 2), chip // 2
+    sib = t + 1 - 2 * core
+    x_peer = t + 2 * (1 - 2 * cx)
+    y_peer = t + 4 * (1 - 2 * cy)
+    xy_peer = t + 2 * (1 - 2 * cx) + 4 * (1 - 2 * cy)
+    first = jnp.where(core == 0, x_peer, y_peer)
+    second = jnp.where(core == 0, y_peer, x_peer)
+
+    barrier = pltpu.get_barrier_semaphore()
+    for peer in (sib, x_peer, y_peer, xy_peer):
+        pl.semaphore_signal(barrier, inc=1, device_id=(z, peer), device_id_type=MESH)
+
+    @pl.when(z >= 1)
+    def _():
+        pl.semaphore_signal(barrier, inc=1, device_id=(z - 1, t), device_id_type=MESH)
+
+    @pl.when(z + 1 < planes)
+    def _():
+        pl.semaphore_signal(barrier, inc=1, device_id=(z + 1, t), device_id_type=MESH)
+
+    ends = jnp.where(z >= 1, 1, 0) + jnp.where(z + 1 < planes, 1, 0)
+    pl.semaphore_wait(barrier, 4 + ends)
+
+    swaps = []
+    for c in range(4):
+        copy = remote(gram_ref.at[c, 1 - core], halves.at[c], h_send.at[c], h_recv.at[c], z, sib)
+        copy.start()
+        swaps.append(copy)
+    for copy in swaps:
+        copy.wait()
+    for c in range(4):
+        part[c] = (gram_ref[c, core] + halves[c]).astype(jnp.bfloat16)
+    sends = []
+    for k, peer in enumerate((xy_peer, x_peer, y_peer)):
+        copy = remote(part.at[peer // 2], landed.at[k], p_send.at[k], p_recv.at[k], z, peer)
+        copy.start()
+        sends.append(copy)
+    own = gram_ref[chip, core] + halves[chip]
+    for copy in sends:
+        copy.wait()
+    for k in range(3):
+        own = own + landed[k].astype(jnp.float32)
+    full_ref[z, t] = own.astype(jnp.bfloat16)
+
+    events = [(0, 0)]
+    for s in range(planes - 1):
+        events += [(1, s), (2, s)]
+
+    def block_of(kind, s):
+        if kind == 0:
+            return z, None
+        if kind == 1:
+            return z - 1 - s, z - 1 - s >= 0
+        return z + 1 + s, z + 1 + s < planes
+
+    def guarded(valid, body):
+        if valid is None:
+            body()
+        else:
+            pl.when(valid)(body)
+
+    def z_copy(direction, s):
+        block = z - s if direction == 0 else z + s
+        target = z + 1 if direction == 0 else z - 1
+        valid = (block >= 0) & (target < planes) if direction == 0 else (block < planes) & (target >= 0)
+        slot = full_ref.at[block, t]
+        return remote(slot, slot, z_send.at[direction, s], z_recv.at[direction, s], target, t), valid
+
+    def a_copy(e, block):
+        slot = full_ref.at[block, t]
+        return remote(slot, slot, a_send.at[e], a_recv.at[e], z, first)
+
+    def b_copy(e, block, k):
+        slot = full_ref.at[block, t if k == 0 else first]
+        return remote(slot, slot, b_send.at[e, k], b_recv.at[e, k], z, second)
+
+    third = jnp.where(core == 0, y_peer, x_peer)
+    fourth = xy_peer
+
+    def d_copy(e, block, k):
+        rank = (t, first, third, fourth)[k]
+        slot = full_ref.at[block, rank]
+        return remote(slot, slot, d_send.at[e, k], d_recv.at[e, k], z, sib)
+
+    def stage_a(e):
+        kind, s = events[e]
+        block, valid = block_of(kind, s)
+
+        def body():
+            if kind == 1:
+                z_copy(0, s)[0].wait_recv()
+            if kind == 2:
+                z_copy(1, s)[0].wait_recv()
+
+        guarded(valid, body)
+        if kind == 0:
+            for direction in (0, 1):
+                copy, ok = z_copy(direction, 0)
+                guarded(ok, copy.start)
+        elif s + 1 < planes - 1:
+            copy, ok = z_copy(kind - 1, s + 1)
+            guarded(ok, copy.start)
+
+        def sends():
+            a_copy(e, block).start()
+            b_copy(e, block, 0).start()
+            d_copy(e, block, 0).start()
+
+        guarded(valid, sends)
+
+    def stage_b(e):
+        block, valid = block_of(*events[e])
+
+        def body():
+            a_copy(e, block).wait_recv()
+            b_copy(e, block, 1).start()
+            d_copy(e, block, 1).start()
+
+        guarded(valid, body)
+
+    def stage_c(e):
+        block, valid = block_of(*events[e])
+
+        def body():
+            b_copy(e, block, 0).wait_recv()
+            d_copy(e, block, 2).start()
+            b_copy(e, block, 1).wait_recv()
+            d_copy(e, block, 3).start()
+
+        guarded(valid, body)
+
+    def stage_d(e):
+        block, valid = block_of(*events[e])
+
+        def body():
+            a_copy(e, block).wait_send()
+            for k in range(2):
+                b_copy(e, block, k).wait_send()
+            for k in range(4):
+                d_copy(e, block, k).wait()
+
+        guarded(valid, body)
+
+    count = len(events)
+    for e in range(count + 3):
+        if e < count:
+            stage_a(e)
+        if 0 <= e - 1 < count:
+            stage_b(e - 1)
+        if 0 <= e - 3 < count:
+            stage_c(e - 3)
+    for e in range(count):
+        stage_d(e)
+    for direction in (0, 1):
+        for s in range(planes - 1):
+            copy, ok = z_copy(direction, s)
+            guarded(ok, copy.wait_send)
+
+
+def sum_and_spread(gram, planes):
+    chips, _, rows, cols = gram.shape
+    vmem = pl.BlockSpec(memory_space=pltpu.VMEM)
+    events = 2 * planes - 1
+    dma = pltpu.SemaphoreType.DMA
+    return pl.pallas_call(
+        functools.partial(spread_kernel, planes),
+        out_shape=jax.ShapeDtypeStruct((planes, 2 * chips, rows, cols), jnp.bfloat16),
+        in_specs=[vmem],
+        out_specs=vmem,
+        scratch_shapes=[
+            pltpu.VMEM((chips, rows, cols), jnp.float32),
+            pltpu.VMEM((chips, rows, cols), jnp.bfloat16),
+            pltpu.VMEM((3, rows, cols), jnp.bfloat16),
+            dma((4,)),
+            dma((4,)),
+            dma((3,)),
+            dma((3,)),
+            dma((2, planes)),
+            dma((2, planes)),
+            dma((events,)),
+            dma((events,)),
+            dma((events, 2)),
+            dma((events, 2)),
+            dma((events, 4)),
+            dma((events, 4)),
+        ],
+        compiler_params=pltpu.CompilerParams(
+            collective_id=2, has_side_effects=True, vmem_limit_bytes=48 << 20
+        ),
+        cost_estimate=pl.CostEstimate(flops=0, bytes_accessed=100 << 20, transcendentals=0),
+    )(gram)
+
+
+def tile_of(rows, most):
+    return max(k for k in range(16, min(rows, most) + 1, 16) if rows % k == 0)
+
+
+def eye_minus_half(current, first_row):
+    at_row = lax.broadcasted_iota(jnp.int32, current.shape, 0) + first_row
+    at_col = lax.broadcasted_iota(jnp.int32, current.shape, 1)
+    return jnp.where(at_row == at_col, 1.5, 0.0) - 0.5 * current
+
+
+def chain_kernel(
+    rows_dev,
+    current_ref,
+    poly_ref,
+    out_ref,
+    square,
+    current1,
+    poly1,
+    square1,
+    poly2,
+    s_send,
+    s_recv,
+    c_send,
+    c_recv,
+    p_send,
+    p_recv,
+    q_send,
+    q_recv,
+):
+    z, t = lax.axis_index("fs"), lax.axis_index("tp")
+    core = lax.rem(t, 2)
+    sib = t + 1 - 2 * core
+    half = current_ref.shape[0] // 2
+    tile = tile_of(half, 352)
+    tiles = half // tile
+    base = core * half
+
+    def rows_of(i):
+        return pl.ds(pl.multiple_of(base + i * tile, 16), tile)
+
+    def share(buffer, send, recv, i):
+        rows = rows_of(i)
+        return remote(buffer.at[rows], buffer.at[rows], send.at[i], recv.at[i], z, sib)
+
+    barrier = pltpu.get_barrier_semaphore()
+    pl.semaphore_signal(barrier, inc=1, device_id=(z, sib), device_id_type=MESH)
+    pl.semaphore_wait(barrier, 1)
+
+    def dot(left, right):
+        return jnp.dot(left, right, preferred_element_type=jnp.float32)
+
+    @pl.loop(0, tiles)
+    def _(i):
+        rows = rows_of(i)
+        square[rows, :] = dot(poly_ref[rows, :], poly_ref[...]).astype(jnp.bfloat16)
+        share(square, s_send, s_recv, i).start()
+
+    for i in range(tiles):
+        share(square, s_send, s_recv, i).wait()
+
+    @pl.loop(0, tiles)
+    def _(i):
+        rows = rows_of(i)
+        value = dot(current_ref[rows, :], square[...])
+        current1[rows, :] = value.astype(jnp.bfloat16)
+        poly1[rows, :] = eye_minus_half(value, base + i * tile).astype(jnp.bfloat16)
+        share(poly1, p_send, p_recv, i).start()
+        share(current1, c_send, c_recv, i).start()
+
+    for i in range(tiles):
+        share(poly1, p_send, p_recv, i).wait()
+        share(current1, c_send, c_recv, i).wait()
+
+    @pl.loop(0, tiles)
+    def _(i):
+        rows = rows_of(i)
+        square[rows, :] = dot(poly_ref[rows, :], poly1[...]).astype(jnp.bfloat16)
+        share(square, q_send, q_recv, i).start()
+
+    small = tile_of(rows_dev, 176)
+    offset = z * rows_dev
+
+    @pl.loop(0, rows_dev // small)
+    def _(i):
+        rows = pl.ds(pl.multiple_of(offset + i * small, 16), small)
+        here = pl.ds(pl.multiple_of(i * small, 16), small)
+        square1[here, :] = dot(poly1[rows, :], poly1[...]).astype(jnp.bfloat16)
+
+    @pl.loop(0, rows_dev // small)
+    def _(i):
+        here = pl.ds(pl.multiple_of(i * small, 16), small)
+        value = dot(square1[here, :], current1[...])
+        poly2[here, :] = eye_minus_half(value, offset + i * small).astype(jnp.bfloat16)
+
+    for i in range(tiles):
+        share(square, q_send, q_recv, i).wait()
+
+    @pl.loop(0, rows_dev // small)
+    def _(i):
+        here = pl.ds(pl.multiple_of(i * small, 16), small)
+        out_ref[here, :] = dot(poly2[here, :], square[...]).astype(jnp.bfloat16)
+
+
+def chain(current_low, poly0, rows_dev):
+    width = current_low.shape[0]
+    vmem = pl.BlockSpec(memory_space=pltpu.VMEM)
+    whole = pltpu.VMEM((width, width), jnp.bfloat16)
+    strip = pltpu.VMEM((rows_dev, width), jnp.bfloat16)
+    tiles = (width // 2) // tile_of(width // 2, 352)
+    return pl.pallas_call(
+        functools.partial(chain_kernel, rows_dev),
+        out_shape=jax.ShapeDtypeStruct((rows_dev, width), jnp.bfloat16),
+        in_specs=[vmem, vmem],
+        out_specs=vmem,
+        scratch_shapes=[whole, whole, whole, strip, strip]
+        + [pltpu.SemaphoreType.DMA((tiles,))] * 8,
+        compiler_params=pltpu.CompilerParams(
+            collective_id=3, has_side_effects=True, vmem_limit_bytes=67043328
+        ),
+        cost_estimate=pl.CostEstimate(
+            flops=4 * width**3, bytes_accessed=100 << 20, transcendentals=0
+        ),
+    )(current_low, poly0)
+
+
+def local(grad_gate, grad_up, moment_gate, moment_up):
+    if grad_gate.shape[0] % 16 or (2 * grad_gate.shape[1]) % 128 or lax.axis_size("tp") != 8 or (grad_gate.shape[0] * lax.axis_size("fs")) % 32:
+        return local_small(grad_gate, grad_up, moment_gate, moment_up)
+    hidden = grad_gate.shape[1] * lax.axis_size("tp")
+    moment_gate_next = BETA * moment_gate + grad_gate
+    moment_up_next = BETA * moment_up + grad_up
+    low = jnp.concatenate(
+        [moment_gate_next.astype(jnp.bfloat16), moment_up_next.astype(jnp.bfloat16)], axis=1
+    )
+    rows_dev = low.shape[0]
+    row_squares = jnp.sum(jnp.square(low.astype(jnp.float32)), axis=1)
+    planes, ranks = lax.axis_size("fs"), lax.axis_size("tp")
+    blocks, shares, vecs = gather_and_gram(low, row_squares[None, :], planes, ranks)
+    columns = blocks.reshape(planes * rows_dev, -1)
+    width = planes * rows_dev
+    diag_gram = jnp.sum(vecs, axis=1).reshape(width)
+    spread = sum_and_spread(shares.reshape(ranks // 2, 2, width // ranks, rows_dev), planes)
+    at_row = lax.broadcasted_iota(jnp.int32, spread.shape, 1) * (
+        width // ranks
+    ) + lax.broadcasted_iota(jnp.int32, spread.shape, 2)
+    at_col = lax.broadcasted_iota(jnp.int32, spread.shape, 0) * rows_dev + (
+        lax.broadcasted_iota(jnp.int32, spread.shape, 3)
+    )
+    square_total = jnp.sum(
+        jnp.where(at_row == at_col, 0.0, jnp.square(spread.astype(jnp.float32)))
+    ) + jnp.sum(jnp.square(diag_gram))
+    trace_total = jnp.sum(diag_gram)
+    spectral = 2.0 * square_total / (trace_total + EPS)
+    gram = spread.transpose(1, 2, 0, 3).reshape(width, width)
+    at_row = lax.broadcasted_iota(jnp.int32, gram.shape, 0)
+    at_col = lax.broadcasted_iota(jnp.int32, gram.shape, 1)
+    current = (
+        jnp.where(at_row == at_col, diag_gram[:, None], gram.astype(jnp.float32)) / spectral
+    )
+    poly0 = (jnp.where(at_row == at_col, 1.5, 0.0) - 0.5 * current).astype(jnp.bfloat16)
+    product = chain(current.astype(jnp.bfloat16), poly0, rows_dev)
+    factor = jnp.sqrt(2.0 * hidden / spectral)
+    ortho = jnp.dot(product, columns, preferred_element_type=jnp.float32) * factor
+    half = grad_gate.shape[1]
+    return (moment_gate_next, moment_up_next, ortho[:, :half], ortho[:, half:])
+
+
 def solution(mesh):
     in_specs = (P("fs", "tp"), P("fs", "tp"), P("fs", "tp"), P("fs", "tp"))
     out_specs = (P("fs", "tp"), P("fs", "tp"), P("fs", "tp"), P("fs", "tp"))

time: 641 us -> 356 us (0.56)
  waiting for transfers between devices: 508 us -> 0 us
  Pallas kernels: 0 us -> 259 us
  matrix products: 47.6 us -> 7.01 us
  blocking collectives: 39.5 us -> 0 us
  local copies, waits for them, and re-layouts: 15.4 us -> 45.3 us
  other arithmetic: 12.4 us -> 40.9 us
  between operations: 16.7 us -> 2.69 us
    all_gather x13 -> x0, waiting for transfers between devices: 451 us -> none  [the longest x5 155 us: multiply(): left_rows = lax.all_gather(left_low, 'fs', axis=1, tiled=True)]
    pallas_call x0 -> x3, Pallas kernels: none -> 259 us  [the longest x1 109 us: gather_and_gram(): pl.pallas_call(functools.partial(gather_kernel, planes, ranks), out_shape...]
    unnamed x15 -> x0, waiting for transfers between devices: 56.5 us -> none
    dot_general x10 -> x1, matrix products: 47.6 us -> 7.01 us  [local(): jnp.dot(product, columns, preferred_element_type=jnp.float32) * factor]
    convert_element_type x0 -> x2, local copies, waits for them, and re-layouts: none -> 40.5 us  [local(): gram.astype(jnp.float32)]
    psum x1 -> x0, blocking collectives: 39.5 us -> none  [local(): lax.psum((trace_local, square_local), ('fs', 'tp'))]
    convert_element_type x0 -> x3, other arithmetic: none -> 28.4 us  [the longest x1 17.3 us: local(): (jnp.where(at_row == at_col, 1.5, 0.0) - 0.5 * current).astype(jnp.bfloat16)]
    all_gather x5 -> x0, local copies, waits for them, and re-layouts: 9.26 us -> none  [multiply(): left_rows = lax.all_gather(left_low, 'fs', axis=1, tiled=True)]
  transfers between devices with their start and end apart: 14 -> 0, of which waited for: 14 -> 0; matrix products, arithmetic and copies ran while one was open for 6% -> 0% of each run, Pallas kernels for 0% -> 0%
where the time goes in v1:
time: 356 us; the launch traced here: 355 us
  Pallas kernels  259 us (73%)
  local copies, waits for them, and re-layouts  45.3 us (13%)
  other arithmetic  40.9 us (11%)
  matrix products  7.01 us (2%)
    pallas_call x1, Pallas kernels, gather_and_gram(): pl.pallas_call(functools.partial(gather_kernel, planes, ranks), out_shape...  109 us
    pallas_call x1, Pallas kernels, sum_and_spread(): pl.pallas_call(functools.partial(spread_kernel, planes), out_shape=jax.Sh...  78.7 us
    pallas_call x1, Pallas kernels, chain(): pl.pallas_call(functools.partial(chain_kernel, rows_dev), out_shape=jax.S...  71.7 us
    convert_element_type x2, local copies, waits for them, and re-layouts, local(): gram.astype(jnp.float32)  40.5 us
    convert_element_type x1, other arithmetic, local(): (jnp.where(at_row == at_col, 1.5, 0.0) - 0.5 * current).astype(jnp.bfloat16)  17.3 us
    reduce_sum x1, other arithmetic, local(): jnp.sum(jnp.where(at_row == at_col, 0.0, jnp.square(spread.astype(jnp.flo...  10.3 us

profile of v1, /device:TPU:0, one launch (start us, length us, event | category | flops | bytes accessed | tf_op | source)
XLA Modules:
  0.0 355.4 jit_solution(9520494785038791762)
XLA Ops:
  0.6 5.1 %fusion.4 = (bf16[528,704]{1,0:T(8,128)(2,1)S(1)}, f32[528,704]{1,0:T(8,128)}, bf16[528,704]{1,0:T(8,128)(2,1)S(1)}, f32[528,704]{1,0:T(8,128)}) fusion(f32[528,704]{1,0:T(8,128)} %param.4, f32[528,704]{1,0:T(8,128)} %param.6, f32[528,704]{1,0:T(8,128)} %param.5, f32[528,704]{1,0:T(8,128)} %param.7), kind=kLoop, calls=%fused_computation.18 | loop fusion | flops 2230272 | bytes 10407936 | tf_op jit(solution)/shard_map/convert_element_type | solution.py:580
  5.7 0.9 multiply_reduce_fusion
  6.6 109.1 %shard_map.75 = (bf16[4,528,1408]{2,1,0:T(8,128)(2,1)S(1)}, f32[4,528,528]{2,1,0:T(8,128)S(1)}, f32[4,8,1,528]{3,2,1,0:T(1,128)S(1)}) custom-call(bf16[528,1408]{1,0:T(8,128)(2,1)S(1)} %get-tuple-element.13.low_ref, f32[1,528]{1,0:T(1,128)S(1)} %broadcast_in_dim.25.vec_ref), custom_call_target="tpu_custom_call" | custom-call | flops 3140222976 | bytes 104857600 | tf_op jit(solution)/shard_map/pallas_call | solution.py:209
  115.7 0.0 copy-start
  115.7 2.5 copy-done
  118.1 78.7 %shard_map.76 = bf16[4,8,264,528]{3,2,1,0:T(8,128)(2,1)} custom-call(f32[4,2,264,528]{3,2,1,0:T(8,128)S(1)} %bitcast.6), custom_call_target="tpu_custom_call" | custom-call | bytes 104857600 | tf_op jit(solution)/shard_map/pallas_call | solution.py:419
  196.8 10.3 %fusion.1 = f32[]{:T(128)} fusion(bf16[4,8,264,528]{3,2,1,0:T(8,128)(2,1)} %shard_map.76, s32[4]{0:T(128)S(1)} %iota_multiply_fusion, s32[8]{0:T(128)S(1)} %iota_multiply_fusion.1), kind=kLoop, calls=%fused_computation.3 | loop fusion | flops 31223808 | bytes 8921140 | tf_op jit(solution)/shard_map/reduce_sum | solution.py:596
  207.1 0.8 fusion.3
  207.9 0.6 multiply_reduce_fusion.1
  210.4 6.1 %convert_bitcast_fusion = f32[8,264,4,528]{3,1,0,2:T(8,128)S(1)} fusion(bf16[4,8,264,528]{3,2,1,0:T(8,128)(2,1)} %shard_map.76), kind=kLoop, calls=%fused_computation.1 | loop fusion | flops 4460544 | bytes 26763264 | tf_op jit(solution)/shard_map/convert_element_type | solution.py:605
  216.5 15.6 %copy.9 = f32[8,264,4,528]{3,2,1,0:T(4,128)} copy(f32[8,264,4,528]{3,1,0,2:T(8,128)S(1)} %convert_bitcast_fusion) | data formatting | bytes 35684352 | tf_op jit(solution)/shard_map/convert_element_type | solution.py:605
  232.1 24.9 %reshape.25 = f32[2112,2112]{1,0:T(8,128)} reshape(f32[8,264,4,528]{3,2,1,0:T(4,128)} %copy.9) | data formatting | bytes 35684352 | tf_op jit(solution)/shard_map/convert_element_type | solution.py:605
  257.0 0.1 broadcast_in_dim.26
  257.1 17.3 %subtract_convert_fusion = (bf16[2112,2112]{1,0:T(8,128)(2,1)}, bf16[2112,2112]{1,0:T(8,128)(2,1)}) fusion(f32[]{:T(128)S(6)} %div.12, f32[2112,2112]{1,0:T(8,128)} %reshape.25, f32[2112]{0:T(1024)S(1)} %broadcast_in_dim.26), kind=kLoop, calls=%fused_computation.5 | loop fusion | flops 35684352 | bytes 35692804 | tf_op jit(solution)/shard_map/convert_element_type | solution.py:607
  274.3 71.7 %shard_map.77 = bf16[528,2112]{1,0:T(8,128)(2,1)} custom-call(bf16[2112,2112]{1,0:T(8,128)(2,1)} %get-tuple-element.19.current_ref, bf16[2112,2112]{1,0:T(8,128)(2,1)} %get-tuple-element.18.poly_ref), custom_call_target="tpu_custom_call" | custom-call | flops 37682675712 | bytes 104857600 | tf_op jit(solution)/shard_map/pallas_call | solution.py:557
  346.1 7.0 %convolution_multiply_fusion = f32[528,1408]{1,0:T(8,128)S(1)} fusion(bf16[528,2112]{1,0:T(8,128)(2,1)} %shard_map.77, bf16[2112,1408]{1,0:T(8,128)(2,1)} %bitcast.7, f32[]{:T(128)S(6)} %sqrt.3), kind=kOutput, calls=%fused_computation.8 | convolution fusion | flops 3140966400 | bytes 11151364 | tf_op jit(solution)/shard_map/dot_general | solution.py:610
  353.1 2.2 fusion.6
  (3 shorter events, 0.0 us)
Async XLA Ops:
  115.7 2.5 copy-start
